TPU v7x, 32 devices: a whole 2x2x4 slice. The times are simulated.
32 devices in a mesh: fs: 8 (over z, y), tp: 4 (over x, core).
Axes of the slice: x: 2, y: 2, z: 4, core: 2. Of those that a mesh axis runs over, the one named last changes fastest.
Arguments:
- inputs: bfloat16 [4608, 2048], P('fs'), may hold values from -6 to 6
- query_cotangent: bfloat16 [4608, 1024], P('fs', 'tp'), may hold values from -0.017944336 to 0.017944336
- value_cotangent: bfloat16 [4608, 1024], P('fs', 'tp'), may hold values from -0.017944336 to 0.017944336
- weights_query: float32 [2048, 1024], P('fs', 'tp'), may hold values from -6 to 6
- weights_value: float32 [2048, 1024], P('fs', 'tp'), may hold values from -6 to 6
- basis_query: bfloat16 [1024, 32], P('tp'), may hold values from -0.75 to 0.75
- basis_value: bfloat16 [1024, 32], P('tp'), may hold values from -0.75 to 0.75
- first_query: float32 [2048, 512], P('fs', 'tp'), may hold values from -5.4 to 5.4, as said below
- second_query: float32 [2048, 512], P('fs', 'tp'), may hold values from 0.05 to 1
- first_value: float32 [2048, 512], P('fs', 'tp'), may hold values from -5.4 to 5.4, as said below
- second_value: float32 [2048, 512], P('fs', 'tp'), may hold values from 0.05 to 1
Outputs:
- step_query: float32 [2048, 1024], P('fs', 'tp')
- step_value: float32 [2048, 1024], P('fs', 'tp')
- new_query: float32 [2048, 1024], P('fs', 'tp')
- new_value: float32 [2048, 1024], P('fs', 'tp')
- copy_query: bfloat16 [2048, 1024], P(None, 'tp')
- copy_value: bfloat16 [2048, 1024], P(None, 'tp')
- moment_query: float32 [2048, 512], P('fs', 'tp')
- square_query: float32 [2048, 512], P('fs', 'tp')
- moment_value: float32 [2048, 512], P('fs', 'tp')
- square_value: float32 [2048, 512], P('fs', 'tp')
Inputs may be any that keep to these rules, and one draw needn't show every extreme that they name: `first_query`: first moments, with a spread of scale from row to row. `first_value`: first moments, with a spread of scale from row to row.
All inputs are finite; a program needn't handle non-finite values.
Results may differ from a plain program's by a relative error of at most 0.003.
Values may be sent and summed in bfloat16 or wider, within the bound.
A program may use at most 64 MiB of HBM per device.

v0:
```python
import functools

import jax
import jax.numpy as jnp
from jax import lax
from jax.experimental import pallas as pl
from jax.experimental.pallas import tpu as pltpu
from jax.sharding import PartitionSpec as P

HEAD = 64
RK = 32
MESH = pl.DeviceIdType.MESH
F32 = jnp.float32
BF16 = jnp.bfloat16


def flip(x, bits):
    out, weight = x, 1
    while weight <= bits:
        if bits & weight:
            out = out + weight * (1 - 2 * ((x // weight) % 2))
        weight *= 2
    return out


def remote(src, dst, send, recv, to):
    return pltpu.make_async_remote_copy(
        src_ref=src, dst_ref=dst, send_sem=send, recv_sem=recv, device_id=to, device_id_type=MESH
    )


def body(
    n,
    t,
    x_hbm,
    cq_hbm,
    cv_hbm,
    wq_hbm,
    wv_hbm,
    bq_hbm,
    bv_hbm,
    fq_hbm,
    sq_hbm,
    fv_hbm,
    sv_hbm,
    step,
    new,
    copy,
    mom,
    sqr,
    x,
    cot,
    w,
    basis,
    first,
    second,
    small,
    part,
    summed,
    arrived1,
    arrived2,
    raw,
    tot,
    tot_all,
    in_sem,
    s1,
    r1,
    s2,
    r2,
    st,
    rt,
    su,
    ru,
    sd,
    rd,
    sy,
    ry,
    sn,
    rn,
):
    f = lax.axis_index("fs")
    g = lax.axis_index("tp")
    me = f * t + g
    count = n * t
    outer = n // 2
    a, b = f // 2, f % 2
    mate = (a * 2 + 1 - b, g)
    depth = x.shape[1]
    rows = depth // n
    cols = w.shape[2]
    wide = cols // HEAD * RK

    barrier = pltpu.get_barrier_semaphore()

    def greet(i, c):
        j = (me + 1 + i) % count
        pl.semaphore_signal(barrier, inc=1, device_id=(j // t, j % t), device_id_type=MESH)
        return c

    lax.fori_loop(0, count - 1, greet, 0)

    loads = [
        pltpu.make_async_copy(src, dst, in_sem.at[i])
        for i, (src, dst) in enumerate(
            (
                (bq_hbm, basis.at[0]),
                (bv_hbm, basis.at[1]),
                (cq_hbm, cot.at[0]),
                (cv_hbm, cot.at[1]),
                (x_hbm, x),
                (fq_hbm, first.at[0]),
                (fv_hbm, first.at[1]),
                (sq_hbm, second.at[0]),
                (sv_hbm, second.at[1]),
                (wq_hbm, w.at[0]),
                (wv_hbm, w.at[1]),
            )
        )
    ]
    for load in loads:
        load.start()
    for load in loads[:4]:
        load.wait()

    spread = (
        lax.broadcasted_iota(jnp.int32, (RK, wide), 1) % RK
        == lax.broadcasted_iota(jnp.int32, (RK, wide), 0)
    ).astype(BF16)
    own_head = (
        lax.broadcasted_iota(jnp.int32, (cols, wide), 0) // HEAD
        == lax.broadcasted_iota(jnp.int32, (cols, wide), 1) // RK
    )
    diag = [
        jnp.where(
            own_head,
            lax.dot_general(basis[p], spread, (((0,), (0,)), ((), ())), preferred_element_type=F32),
            0.0,
        ).astype(BF16)
        for p in range(2)
    ]
    for p in range(2):
        small[:, p * wide : (p + 1) * wide] = jnp.dot(
            cot[p], diag[p], preferred_element_type=F32
        ).astype(BF16)
    loads[4].wait()

    chunk = max(2 * rows, min(depth, 256))
    chunks = depth // chunk
    pairs = chunk // (2 * rows)
    order = list(range(chunks // 2, chunks)) + list(range(chunks // 2 - 1, -1, -1))
    at = a // pairs

    def part_rows(z, half):
        return pl.ds(pl.multiple_of((z * 2 + half) * rows, rows), rows)

    def first_copy(k, i, p):
        z = flip(at, order[k]) * pairs + i
        return remote(
            part.at[p, part_rows(z, 1 - b)],
            arrived1.at[p, z],
            s1.at[k * pairs + i, p],
            r1.at[k * pairs + i, p],
            mate,
        )

    for k in range(chunks):
        here = pl.ds(pl.multiple_of(flip(at, order[k]) * chunk, chunk), chunk)
        sums = lax.dot_general(
            x[:, here], small[...], (((0,), (0,)), ((), ())), preferred_element_type=F32
        ).astype(BF16)
        for p in range(2):
            part[p, here] = sums[:, p * wide : (p + 1) * wide]
        if k == 0:
            pl.semaphore_wait(barrier, count - 1)
        for i in range(pairs):
            first_copy(k, i, 0).start()
    for k in range(chunks):
        for i in range(pairs):
            first_copy(k, i, 1).start()

    def second_copy(k, i, p):
        z = flip(at, order[k]) * pairs + i
        return z, remote(
            summed.at[p, z],
            arrived2.at[p, a],
            s2.at[k * pairs + i, p],
            r2.at[a, p],
            (z * 2 + b, g),
        )

    def total_copy(i, p):
        j = (me + 1 + i) % count
        return remote(
            tot.at[p, 0], tot_all.at[p, me], st.at[p, i], rt.at[p, me], (j // t, j % t)
        )

    back = (((1,), (1,)), ((), ()))

    def reduce(p):
        for k in range(chunks):
            for i in range(pairs):
                first_copy(k, i, p).wait_recv()
                if k < chunks - 1 or pairs > 1:
                    z, onward = second_copy(k, i, p)
                    summed[p, z] = (
                        part[p, part_rows(z, b)].astype(F32) + arrived1[p, z].astype(F32)
                    ).astype(BF16)
                    if k < chunks - 1:
                        onward.start()
                    else:
                        pl.when(z != a)(onward.start)
        reduced = part[p, part_rows(a, b)].astype(F32) + arrived1[p, a].astype(F32)
        for q in range(outer - 1, 0, -1):
            src = flip(a, q)
            remote(
                summed.at[p, src],
                arrived2.at[p, src],
                s2.at[0, p],
                r2.at[src, p],
                (src * 2 + b, g),
            ).wait_recv()
            reduced = reduced + arrived2[p, src].astype(F32)
        if p == 0:
            for load in loads[5:]:
                load.wait()
        moment = 0.9 * first[p] + 0.1 * reduced
        square = 0.95 * second[p] + 0.05 * reduced * reduced
        direction = moment / (jnp.sqrt(square) + 1e-08)
        tot[p, 0] = jnp.sum(direction * direction, axis=0, keepdims=True)

        def send_total(i, c):
            total_copy(i, p).start()
            return c

        lax.fori_loop(0, count - 1, send_total, 0)
        tot_all[p, me] = tot[p, 0]
        mom[p] = moment
        sqr[p] = square
        upper = direction.astype(BF16)
        lower = (direction - upper.astype(F32)).astype(BF16)
        raw[p] = lax.dot_general(upper, diag[p], back, preferred_element_type=F32) + lax.dot_general(
            lower, diag[p], back, preferred_element_type=F32
        )

    entries = depth * wide * t

    def block(z, half):
        return pl.ds(pl.multiple_of((z * 2 + half) * rows, rows), rows)

    up_to, down_to = (f + 2, g), (f - 2, g)

    def up(k, p):
        rows_at = block(a - k, b)
        ref = copy.at[p, rows_at]
        return remote(ref, ref, su.at[k, p], ru.at[k, p], up_to)

    def down(k, p):
        ref = copy.at[p, block(a + k, b)]
        return remote(ref, ref, sd.at[k, p], rd.at[k, p], down_to)

    def up_in(k, p):
        ref = copy.at[p, block(a - 1 - k, b)]
        return remote(ref, ref, su.at[k, p], ru.at[k, p], up_to)

    def down_in(k, p):
        ref = copy.at[p, block(a + 1 + k, b)]
        return remote(ref, ref, sd.at[k, p], rd.at[k, p], down_to)

    def across(z, p):
        ref = copy.at[p, block(z, b)]
        return remote(ref, ref, sy.at[z, p], ry.at[z, p], mate)

    def across_in(z, p):
        ref = copy.at[p, block(z, 1 - b)]
        return remote(ref, ref, sy.at[z, p], ry.at[z, p], mate)

    near = flip(a, 1)

    def beside(z):
        ref = copy.at[1, block(z, 1 - b)]
        return remote(ref, ref, sn.at[0], rn.at[0], (near * 2 + b, g))

    def finish(p):
        def await_total(i, c):
            j = (me + 1 + i) % count
            remote(
                tot.at[p, 0], tot_all.at[p, j], st.at[p, i], rt.at[p, j], (j // t, j % t)
            ).wait_recv()
            return c

        lax.fori_loop(0, count - 1, await_total, 0)
        mean = jnp.sum(jnp.sum(tot_all[p], axis=0), axis=1, keepdims=True) / entries
        scale = 1.0 / jnp.sqrt(mean + 0.25)
        move = scale * raw[p]
        fresh = w[p] - 0.1 * move
        copy[p, block(a, b)] = fresh.astype(BF16)
        pl.when(a < outer - 1)(lambda: up(0, p).start())
        pl.when(a > 0)(lambda: down(0, p).start())
        across(a, p).start()
        step[p] = move
        new[p] = fresh

    def forward(k, p):
        @pl.when(a - 1 - k >= 0)
        def _():
            up_in(k, p).wait_recv()
            if k + 1 < outer - 1:
                pl.when(a < outer - 1)(lambda: up(k + 1, p).start())
            if k == 0 and p == 1:
                pl.when(a % 2 == 0)(lambda: across(a - 1, p).start())
            else:
                across(a - 1 - k, p).start()

        @pl.when(a + 1 + k <= outer - 1)
        def _():
            down_in(k, p).wait_recv()
            if k + 1 < outer - 1:
                pl.when(a > 0)(lambda: down(k + 1, p).start())
            if k == 0 and p == 1:
                pl.when(a % 2 == 1)(lambda: across(a + 1, p).start())
            else:
                across(a + 1 + k, p).start()

    reduce(0)
    reduce(1)
    finish(0)
    forward(0, 0)
    finish(1)
    for k in range(outer - 1):
        if k + 1 < outer - 1:
            forward(k + 1, 0)
        forward(k, 1)
        if k == 0:
            across_in(a, 1).wait_recv()
            beside(a).start()

    for z in range(outer):
        for p in range(2):
            if p == 0:
                across_in(z, p).wait_recv()
                across(z, p).wait_send()
            else:
                pl.when(jnp.logical_and(z != near, z != a))(lambda: across_in(z, 1).wait_recv())
                pl.when(z != near)(lambda: across(z, 1).wait_send())
    beside(near).wait_recv()
    beside(a).wait_send()

    for p in range(2):
        for k in range(chunks):
            for i in range(pairs):
                first_copy(k, i, p).wait_send()
                if k < chunks - 1:
                    second_copy(k, i, p)[1].wait_send()
                elif pairs > 1:
                    z, onward = second_copy(k, i, p)
                    pl.when(z != a)(onward.wait_send)

        def sent_total(i, c):
            total_copy(i, p).wait_send()
            return c

        lax.fori_loop(0, count - 1, sent_total, 0)
        for k in range(outer - 1):
            pl.when(jnp.logical_and(a - k >= 0, a < outer - 1))(lambda: up(k, p).wait_send())
            pl.when(jnp.logical_and(a + k <= outer - 1, a > 0))(lambda: down(k, p).wait_send())


def store(step, new, copy, mom, sqr, *rest):
    outs, sem = rest[:10], rest[10]
    srcs = [ref.at[p] for ref in (step, new, copy, mom, sqr) for p in range(2)]
    order = (4, 5, 0, 1, 2, 3, 6, 7, 8, 9)
    moves = [pltpu.make_async_copy(srcs[i], outs[i], sem.at[i]) for i in order]
    for move in moves:
        move.start()
    for move in moves:
        move.wait()


def per_device(n, t, x, cq, cv, wq, wv, bq, bv, fq, sq, fv, sv):
    tokens, depth = x.shape
    rows, cols = wq.shape
    wide = fq.shape[1]
    outer = n // 2
    hbm = pl.BlockSpec(memory_space=pltpu.HBM)
    vmem = pl.BlockSpec(memory_space=pltpu.VMEM)
    shape = jax.ShapeDtypeStruct
    dma = pltpu.SemaphoreType.DMA
    kept = (
        pltpu.VMEM((2, rows, cols), F32),
        pltpu.VMEM((2, rows, cols), F32),
        pltpu.VMEM((2, depth, cols), BF16),
        pltpu.VMEM((2, rows, wide), F32),
        pltpu.VMEM((2, rows, wide), F32),
    )
    held = pl.pallas_call(
        functools.partial(body, n, t),
        out_shape=kept,
        in_specs=[hbm] * 11,
        out_specs=[vmem] * 5,
        scratch_shapes=[
            pltpu.VMEM((tokens, depth), BF16),
            pltpu.VMEM((2, tokens, cols), BF16),
            pltpu.VMEM((2, rows, cols), F32),
            pltpu.VMEM((2, RK, cols), BF16),
            pltpu.VMEM((2, rows, wide), F32),
            pltpu.VMEM((2, rows, wide), F32),
            pltpu.VMEM((tokens, 2 * wide), BF16),
            pltpu.VMEM((2, depth, wide), BF16),
            pltpu.VMEM((2, outer, rows, wide), BF16),
            pltpu.VMEM((2, outer, rows, wide), BF16),
            pltpu.VMEM((2, outer, rows, wide), BF16),
            pltpu.VMEM((2, rows, cols), F32),
            pltpu.VMEM((2, 1, 1, wide), F32),
            pltpu.VMEM((2, n * t, 1, wide), F32),
            dma((11,)),
            dma((outer, 2)),
            dma((outer, 2)),
            dma((outer, 2)),
            dma((outer, 2)),
            dma((2, n * t)),
            dma((2, n * t)),
            dma((outer, 2)),
            dma((outer, 2)),
            dma((outer, 2)),
            dma((outer, 2)),
            dma((outer, 2)),
            dma((outer, 2)),
            dma((1,)),
            dma((1,)),
        ],
        compiler_params=pltpu.CompilerParams(
            collective_id=0, has_side_effects=True, vmem_limit_bytes=62 * 10**6
        ),
        name="update",
    )(x, cq, cv, wq, wv, bq.T, bv.T, fq, sq, fv, sv)
    full, half = shape((rows, cols), F32), shape((rows, wide), F32)
    whole = shape((depth, cols), BF16)
    outs = pl.pallas_call(
        store,
        out_shape=(full,) * 4 + (whole,) * 2 + (half,) * 4,
        in_specs=[vmem] * 5,
        out_specs=[hbm] * 10,
        scratch_shapes=[dma((10,))],
        compiler_params=pltpu.CompilerParams(vmem_limit_bytes=40 * 2**20),
        name="store",
    )(*held)
    return tuple(outs[i] for i in (0, 1, 2, 3, 4, 5, 6, 8, 7, 9))


def solution(mesh):
    split = P("fs", "tp")
    return jax.shard_map(
        functools.partial(per_device, mesh.shape["fs"], mesh.shape["tp"]),
        mesh=mesh,
        in_specs=(P("fs", None),) + (split,) * 4 + (P("tp", None),) * 2 + (split,) * 4,
        out_specs=(split,) * 4 + (P(None, "tp"),) * 2 + (split,) * 4,
        check_vma=False,
    )
```

profile of v0, /device:TPU:0, one launch (start us, length us, event | category | flops | bytes accessed | tf_op | source)
XLA Modules:
  0.0 58.4 jit_solution(1187219184506320546)
XLA Ops:
  0.6 55.8 %update.1 = (f32[2,256,256]{2,1,0:T(8,128)S(1)}, f32[2,256,256]{2,1,0:T(8,128)S(1)}, bf16[2,2048,256]{2,1,0:T(8,128)(2,1)S(1)}, f32[2,256,128]{2,1,0:T(8,128)S(1)}, f32[2,256,128]{2,1,0:T(8,128)S(1)}) custom-call(bf16[576,2048]{1,0:T(8,128)(2,1)} %x_hbm.1, bf16[576,256]{1,0:T(8,128)(2,1)} %cq_hbm.1, bf16[576,256]{1,0:T(8,128)(2,1)} %cv_hbm.1, ...), custom_call_target="tpu_custom_call" | custom-call | tf_op jit(solution)/shard_map/update/pallas_call | solution.py:395
  56.4 1.9 %store.1 = (f32[256,256]{1,0:T(8,128)}, f32[256,256]{1,0:T(8,128)}, f32[256,256]{1,0:T(8,128)}, f32[256,256]{1,0:T(8,128)}, bf16[2048,256]{1,0:T(8,128)(2,1)}, /...) custom-call(f32[2,256,256]{2,1,0:T(8,128)S(1)} %get-tuple-element.25, ...), custom_call_target="tpu_custom_call" | custom-call | tf_op jit(solution)/shard_map/store/pallas_call | solution.py:438
where the time goes:
time: 58.6 us; the launch traced here: 58.4 us
  Pallas kernels  57.7 us (98%)
  between operations  0.65 us (1%)
    pallas_call x1, Pallas kernels, per_device(): pl.pallas_call(functools.partial(body, n, t), out_shape=kept, in_specs=[h...  55.8 us
    pallas_call x1, Pallas kernels, per_device(): pl.pallas_call(store, out_shape=(full,) * 4 + (whole,) * 2 + (half,) * 4,...  1.91 us

commit v1 on v0

v1 whole, which is shorter than its diff:
```python
import functools

import jax
import jax.numpy as jnp
from jax import lax
from jax.experimental import pallas as pl
from jax.experimental.pallas import tpu as pltpu
from jax.sharding import PartitionSpec as P

HEAD = 64
RK = 32
CUT = 2
MESH = pl.DeviceIdType.MESH
F32 = jnp.float32
BF16 = jnp.bfloat16


def flip(x, bits):
    out, weight = x, 1
    while weight <= bits:
        if bits & weight:
            out = out + weight * (1 - 2 * ((x // weight) % 2))
        weight *= 2
    return out


def remote(src, dst, send, recv, to):
    return pltpu.make_async_remote_copy(
        src_ref=src, dst_ref=dst, send_sem=send, recv_sem=recv, device_id=to, device_id_type=MESH
    )


def body(
    n,
    t,
    x_hbm,
    cq_hbm,
    cv_hbm,
    wq_hbm,
    wv_hbm,
    bq_hbm,
    bv_hbm,
    fq_hbm,
    sq_hbm,
    fv_hbm,
    sv_hbm,
    step,
    new,
    copy,
    mom,
    sqr,
    x,
    cot,
    w,
    basis,
    first,
    second,
    small,
    part,
    summed,
    arrived1,
    arrived2,
    raw,
    tot,
    tot_all,
    in_sem,
    x_sem,
    s1,
    r1,
    s2,
    r2,
    st,
    rt,
    so,
    sr,
    rz,
    sy,
    ry,
    sn,
    rn,
    rm,
):
    f = lax.axis_index("fs")
    g = lax.axis_index("tp")
    me = f * t + g
    count = n * t
    outer = n // 2
    a, b = f // 2, f % 2
    mate = (a * 2 + 1 - b, g)
    depth = x.shape[1]
    rows = depth // n
    cols = w.shape[2]
    wide = cols // HEAD * RK
    cut = rz.shape[2]
    bit = rows // cut

    chunk = max(2 * rows, min(depth, 256))
    chunks = depth // chunk
    pairs = chunk // (2 * rows)
    order = list(range(chunks // 2, chunks)) + list(range(chunks // 2 - 1, -1, -1))
    at = a // pairs

    def chunk_at(k):
        return pl.ds(pl.multiple_of(flip(at, order[k]) * chunk, chunk), chunk)

    sources = ((bq_hbm, bv_hbm), (cq_hbm, cv_hbm), (fq_hbm, fv_hbm), (sq_hbm, sv_hbm), (wq_hbm, wv_hbm))
    holders = (basis, cot, first, second, w)

    def load(i):
        for p in range(2):
            pltpu.make_async_copy(sources[i][p], holders[i].at[p], in_sem.at[i]).start()

    def loaded(i):
        pltpu.make_async_copy(holders[i], holders[i], in_sem.at[i]).wait()

    x_loads = [
        pltpu.make_async_copy(x_hbm.at[:, chunk_at(k)], x.at[:, chunk_at(k)], x_sem.at[k])
        for k in range(chunks)
    ]
    load(0)
    load(1)
    x_loads[0].start()

    barrier = pltpu.get_barrier_semaphore()

    def hello(to):
        pl.semaphore_signal(barrier, inc=1, device_id=to, device_id_type=MESH)

    def greet_line(i, c):
        hello(((a + 1 + i) % outer * 2 + b, g))
        return c

    hello(mate)
    lax.fori_loop(0, outer - 1, greet_line, 0)
    for i in range(1, t):
        hello((f, (g + i) % t))
    for x_load in x_loads[1:]:
        x_load.start()
    for i in range(2, 5):
        load(i)
    loaded(0)

    spread = (
        lax.broadcasted_iota(jnp.int32, (RK, wide), 1) % RK
        == lax.broadcasted_iota(jnp.int32, (RK, wide), 0)
    ).astype(BF16)
    own_head = (
        lax.broadcasted_iota(jnp.int32, (cols, wide), 0) // HEAD
        == lax.broadcasted_iota(jnp.int32, (cols, wide), 1) // RK
    )
    diag = [
        jnp.where(
            own_head,
            lax.dot_general(basis[p], spread, (((0,), (0,)), ((), ())), preferred_element_type=F32),
            0.0,
        ).astype(BF16)
        for p in range(2)
    ]
    loaded(1)
    for p in range(2):
        small[:, p * wide : (p + 1) * wide] = jnp.dot(
            cot[p], diag[p], preferred_element_type=F32
        ).astype(BF16)

    def block(z, half):
        return pl.ds(pl.multiple_of((z * 2 + half) * rows, rows), rows)

    def first_copy(k, i, p):
        z = flip(at, order[k]) * pairs + i
        return remote(
            part.at[p, block(z, 1 - b)],
            arrived1.at[p, z],
            s1.at[p],
            r1.at[k * pairs + i, p],
            mate,
        )

    def multiply(here):
        sums = lax.dot_general(
            x[:, here], small[...], (((0,), (0,)), ((), ())), preferred_element_type=F32
        ).astype(BF16)
        for p in range(2):
            part[p, here] = sums[:, p * wide : (p + 1) * wide]

    apart = rows % 128 == 0
    for k in range(chunks):
        x_loads[k].wait()
        multiply(block(flip(at, order[k]), 1 - b) if apart else chunk_at(k))
        if k == 0:
            pl.semaphore_wait(barrier, outer + t - 1)
        for i in range(pairs):
            first_copy(k, i, 0).start()
    for k in range(chunks):
        for i in range(pairs):
            first_copy(k, i, 1).start()
    if apart:
        for k in range(chunks):
            multiply(block(flip(at, order[k]), b))

    def onward(k, p):
        for i in range(pairs):
            first_copy(k, i, p).wait_recv()
            if k < chunks - 1 or pairs > 1:
                z = flip(at, order[k]) * pairs + i
                send = remote(
                    summed.at[p, z], arrived2.at[p, a], s2.at[p], r2.at[p], (z * 2 + b, g)
                )
                summed[p, z] = (
                    part[p, block(z, b)].astype(F32) + arrived1[p, z].astype(F32)
                ).astype(BF16)
                if k < chunks - 1:
                    send.start()
                else:
                    pl.when(z != a)(send.start)

    def others(ref, p):
        return ref.at[p, pl.ds(0, outer - 1)]

    back = (((1,), (1,)), ((), ()))

    def gather(p):
        reduced = part[p, block(a, b)].astype(F32) + arrived1[p, a].astype(F32)
        remote(others(summed, p), others(arrived2, p), s2.at[p], r2.at[p], mate).wait_recv()
        for q in range(outer - 1, 0, -1):
            reduced = reduced + arrived2[p, flip(a, q)].astype(F32)
        if p == 0:
            for i in range(2, 5):
                loaded(i)
        moment = 0.9 * first[p] + 0.1 * reduced
        square = 0.95 * second[p] + 0.05 * reduced * reduced
        direction = moment / (jnp.sqrt(square) + 1e-08)
        tot[p, 0] = jnp.sum(direction * direction, axis=0, keepdims=True)

        def send_total(to):
            remote(tot.at[p, 0], tot_all.at[p, me], st.at[p], rt.at[p], to).start()

        def send_row(i, c):
            to = f + n // 2 + i
            to = to - n * (to // n)
            for h in range(t):
                send_total((to, h))
            return c

        lax.fori_loop(0, n // 2, send_row, 0)
        lax.fori_loop(n // 2 + 1, n, send_row, 0)
        for i in range(1, t):
            send_total((f, (g + i) % t))
        tot_all[p, me] = tot[p, 0]
        mom[p] = moment
        sqr[p] = square
        upper = direction.astype(BF16)
        lower = (direction - upper.astype(F32)).astype(BF16)
        raw[p] = lax.dot_general(upper, diag[p], back, preferred_element_type=F32) + lax.dot_general(
            lower, diag[p], back, preferred_element_type=F32
        )

    entries = depth * wide * t

    def all_totals(p):
        ref = tot_all.at[p, pl.ds(0, count - 1)]
        return remote(ref, ref, st.at[p], rt.at[p], mate)

    def piece(z, half, p, h):
        return copy.at[p, pl.ds(pl.multiple_of((z * 2 + half) * rows + h * bit, bit), bit)]

    def line_copy(z, p, h, sem, to):
        ref = piece(z, b, p, h)
        return remote(ref, ref, sem, rz.at[z, p, h], (to * 2 + b, g))

    def across(z, half, p, h):
        ref = piece(z, half, p, h)
        return remote(ref, ref, sy.at[p], ry.at[p], mate)

    def own_across(half, h):
        ref = piece(a, half, 1, h)
        return remote(ref, ref, sy.at[1], rm.at[h], mate)

    def crossed(p, blocks):
        ref = copy.at[p, pl.ds(0, blocks * rows)]
        return remote(ref, ref, sy.at[p], ry.at[p], mate)

    near = flip(a, 1)

    def beside(z, h):
        ref = piece(z, 1 - b, 1, h)
        return remote(ref, ref, sn.at[0], rn.at[0], (near * 2 + b, g))

    def whole_beside():
        ref = copy.at[1, block(a, b)]
        return remote(ref, ref, sn.at[0], rn.at[0], mate)

    def own_ways():
        for i, d in enumerate((2, -2, 1, -1)):
            yield i, d, a + d <= outer - 1 if d > 0 else a + d >= 0

    def finish(p):
        all_totals(p).wait_recv()
        mean = jnp.sum(jnp.sum(tot_all[p], axis=0), axis=1, keepdims=True) / entries
        scale = 1.0 / jnp.sqrt(mean + 0.25)
        move = scale * raw[p]
        fresh = w[p] - 0.1 * move
        copy[p, block(a, b)] = fresh.astype(BF16)
        for h in range(cut):
            for i, d, ok in own_ways():
                pl.when(ok)(line_copy(a, p, h, so.at[i, p], a + d).start)
            (own_across(b, h) if p else across(a, b, p, h)).start()
        step[p] = move
        new[p] = fresh

    def whole(z, p, sem):
        ref = copy.at[p, block(z, b)]
        return remote(ref, ref, sem, rn.at[0], mate)

    def relays(far):
        up = far > 0
        return (a < outer - 1 if up else a > 0), (sr.at[int(up), abs(far) - 2]), a + (1 if up else -1)

    def forward(d, p, h):
        for far in (d, -d):
            z = a - far

            def handle(far=far, z=z):
                line_copy(z, p, h, sn.at[0], a).wait_recv()
                if 2 <= d < outer - 1:
                    ok, sem, to = relays(far)
                    pl.when(ok)(line_copy(z, p, h, sem.at[p], to).start)
                if d == 1 and p == 1:
                    pl.when(z != near)(lambda: across(z, b, p, h).start())
                else:
                    across(z, b, p, h).start()

            pl.when(z >= 0 if far > 0 else z <= outer - 1)(handle)

    def sent(p):
        remote(arrived1.at[p], arrived1.at[p], s1.at[p], r1.at[0, p], mate).wait_send()
        remote(others(summed, p), others(arrived2, p), s2.at[p], r2.at[p], mate).wait_send()
        all_totals(p).wait_send()

    def sent_copies(p):
        for i, d, ok in own_ways():
            pl.when(ok)(whole(a, p, so.at[i, p]).wait_send)
        for d in range(2, outer - 1):
            for far in (d, -d):
                ok, sem, _ = relays(far)
                z = a - far
                there = z >= 0 if far > 0 else z <= outer - 1
                pl.when(jnp.logical_and(ok, there))(whole(z, p, sem.at[p]).wait_send)
        crossed(p, outer - p).wait_send()

    for k in range(chunks):
        onward(k, 0)
    onward(0, 1)
    gather(0)
    for k in range(1, chunks):
        onward(k, 1)
    gather(1)
    finish(0)

    def due(d, p, h):
        return 4.7 * p + (4.5 + 1.4 * h if d == 1 else 5.2 + 4 * (d - 2) + 3.8 * h)

    def pass_on(h):
        own_across(1 - b, h).wait_recv()
        beside(a, h).start()

    todo = [(4.6, lambda: finish(1)), (9, lambda: sent(0)), (9, lambda: sent(1))]
    for h in range(cut):
        for d in range(1, outer):
            for p in range(2):
                todo.append((due(d, p, h), functools.partial(forward, d, p, h)))
        todo.append((due(2, 1, h) + 0.1, functools.partial(pass_on, h)))
    todo.append((due(outer - 1, 1, cut - 1) - 0.1, lambda: sent_copies(0)))
    for _, act in sorted(todo, key=lambda item: item[0]):
        act()

    crossed(0, outer).wait_recv()
    if outer > 2:
        crossed(1, outer - 2).wait_recv()
    sent_copies(1)
    whole_beside().wait_recv()
    whole_beside().wait_send()


def store(step, new, copy, mom, sqr, *rest):
    outs, sem = rest[:10], rest[10]
    srcs = [ref.at[p] for ref in (step, new, copy, mom, sqr) for p in range(2)]
    order = (4, 5, 0, 1, 2, 3, 6, 7, 8, 9)
    moves = [pltpu.make_async_copy(srcs[i], outs[i], sem.at[i]) for i in order]
    for move in moves:
        move.start()
    for move in moves:
        move.wait()


def per_device(n, t, x, cq, cv, wq, wv, bq, bv, fq, sq, fv, sv):
    tokens, depth = x.shape
    rows, cols = wq.shape
    wide = fq.shape[1]
    outer = n // 2
    chunks = depth // max(2 * rows, min(depth, 256))
    cut = CUT if rows % (16 * CUT) == 0 else 1
    hbm = pl.BlockSpec(memory_space=pltpu.HBM)
    vmem = pl.BlockSpec(memory_space=pltpu.VMEM)
    shape = jax.ShapeDtypeStruct
    dma = pltpu.SemaphoreType.DMA
    kept = (
        pltpu.VMEM((2, rows, cols), F32),
        pltpu.VMEM((2, rows, cols), F32),
        pltpu.VMEM((2, depth, cols), BF16),
        pltpu.VMEM((2, rows, wide), F32),
        pltpu.VMEM((2, rows, wide), F32),
    )
    held = pl.pallas_call(
        functools.partial(body, n, t),
        out_shape=kept,
        in_specs=[hbm] * 11,
        out_specs=[vmem] * 5,
        scratch_shapes=[
            pltpu.VMEM((tokens, depth), BF16),
            pltpu.VMEM((2, tokens, cols), BF16),
            pltpu.VMEM((2, rows, cols), F32),
            pltpu.VMEM((2, RK, cols), BF16),
            pltpu.VMEM((2, rows, wide), F32),
            pltpu.VMEM((2, rows, wide), F32),
            pltpu.VMEM((tokens, 2 * wide), BF16),
            pltpu.VMEM((2, depth, wide), BF16),
            pltpu.VMEM((2, outer, rows, wide), BF16),
            pltpu.VMEM((2, outer, rows, wide), BF16),
            pltpu.VMEM((2, outer, rows, wide), BF16),
            pltpu.VMEM((2, rows, cols), F32),
            pltpu.VMEM((2, 1, 1, wide), F32),
            pltpu.VMEM((2, n * t, 1, wide), F32),
            dma((5,)),
            dma((chunks,)),
            dma((2,)),
            dma((outer, 2)),
            dma((2,)),
            dma((2,)),
            dma((2,)),
            dma((2,)),
            dma((4, 2)),
            dma((2, max(outer - 3, 1), 2)),
            dma((outer, 2, cut)),
            dma((2,)),
            dma((2,)),
            dma((1,)),
            dma((1,)),
            dma((cut,)),
        ],
        compiler_params=pltpu.CompilerParams(
            collective_id=0, has_side_effects=True, vmem_limit_bytes=62 * 10**6
        ),
        name="update",
    )(x, cq, cv, wq, wv, bq.T, bv.T, fq, sq, fv, sv)
    full, half = shape((rows, cols), F32), shape((rows, wide), F32)
    whole = shape((depth, cols), BF16)
    outs = pl.pallas_call(
        store,
        out_shape=(full,) * 4 + (whole,) * 2 + (half,) * 4,
        in_specs=[vmem] * 5,
        out_specs=[hbm] * 10,
        scratch_shapes=[dma((10,))],
        compiler_params=pltpu.CompilerParams(vmem_limit_bytes=40 * 2**20),
        name="store",
    )(*held)
    return tuple(outs[i] for i in (0, 1, 2, 3, 4, 5, 6, 8, 7, 9))


def solution(mesh):
    split = P("fs", "tp")
    return jax.shard_map(
        functools.partial(per_device, mesh.shape["fs"], mesh.shape["tp"]),
        mesh=mesh,
        in_specs=(P("fs", None),) + (split,) * 4 + (P("tp", None),) * 2 + (split,) * 4,
        out_specs=(split,) * 4 + (P(None, "tp"),) * 2 + (split,) * 4,
        check_vma=False,
    )
```

time: 58.6 us -> 51 us (0.87)
  Pallas kernels: 57.7 us -> 50.1 us
    pallas_call x1, Pallas kernels: 55.8 us -> 48.2 us  [per_device(): pl.pallas_call(functools.partial(body, n, t), out_shape=kept, in_specs=[h...]
where the time goes in v1:
time: 51 us; the launch traced here: 50.7 us
  Pallas kernels  50.1 us (98%)
  between operations  0.65 us (1%)
    pallas_call x1, Pallas kernels, per_device(): pl.pallas_call(functools.partial(body, n, t), out_shape=kept, in_specs=[h...  48.2 us
    pallas_call x1, Pallas kernels, per_device(): pl.pallas_call(store, out_shape=(full,) * 4 + (whole,) * 2 + (half,) * 4,...  1.91 us

profile of v1, /device:TPU:0, one launch (start us, length us, event | category | flops | bytes accessed | tf_op | source)
XLA Modules:
  0.0 50.7 jit_solution(4096543571753032206)
XLA Ops:
  0.6 48.2 %update.1 = (f32[2,256,256]{2,1,0:T(8,128)S(1)}, f32[2,256,256]{2,1,0:T(8,128)S(1)}, bf16[2,2048,256]{2,1,0:T(8,128)(2,1)S(1)}, f32[2,256,128]{2,1,0:T(8,128)S(1)}, f32[2,256,128]{2,1,0:T(8,128)S(1)}) custom-call(bf16[576,2048]{1,0:T(8,128)(2,1)} %x_hbm.1, bf16[576,256]{1,0:T(8,128)(2,1)} %cq_hbm.1, bf16[576,256]{1,0:T(8,128)(2,1)} %cv_hbm.1, ...), custom_call_target="tpu_custom_call" | custom-call | tf_op jit(solution)/shard_map/update/pallas_call | solution.py:413
  48.8 1.9 %store.1 = (f32[256,256]{1,0:T(8,128)}, f32[256,256]{1,0:T(8,128)}, f32[256,256]{1,0:T(8,128)}, f32[256,256]{1,0:T(8,128)}, bf16[2048,256]{1,0:T(8,128)(2,1)}, /...) custom-call(f32[2,256,256]{2,1,0:T(8,128)S(1)} %get-tuple-element.25, ...), custom_call_target="tpu_custom_call" | custom-call | tf_op jit(solution)/shard_map/store/pallas_call | solution.py:457

commit v2 on v1

--- a/solution.py
+++ b/solution.py
@@ -10,7 +10,30 @@
 HEAD = 64
 RK = 32
 CUT = 2
+FINE = 2
+VSWAP = False
 MESH = pl.DeviceIdType.MESH
+END_PLAN = (
+    ("finish", 0), ("own", "mate", 0, 1), ("own", "mate", 0, 0), ("gather", 1),
+    ("own", "near", 0, 1), ("own", "far", 0, 0), ("pass", "near", 0, 1), ("own", "far", 0, 1),
+    ("pass", "near", 0, 0), ("finish", 1), ("own", "mate", 1, 1), ("own", "mate", 1, 0),
+    ("own", "far", 1, 0), ("own", "near", 0, 0), ("pass", "mid", 0, 0), ("own", "far", 1, 1),
+    ("own", "near", 1, 1), ("pass", "end", 0, 0), ("own", "near", 1, 0), ("pass", "mid", 1, 0),
+    ("pass", "near", 1, 1), ("beside", 0), ("pass", "end", 0, 1), ("pass", "end", 1, 0),
+    ("beside", 1), ("pass", "mid", 0, 1), ("pass", "mid", 1, 1), ("pass", "end", 1, 1),
+    ("pass", "near", 1, 0),
+)
+MIDDLE_PLAN = (
+    ("finish", 0), ("own", "mate", 0, 0), ("own", "mate", 0, 1), ("gather", 1),
+    ("own", "near", 0, 1), ("own", "inner", 0, 0), ("own", "near", 0, 0), ("pass", "inner", 0, 0),
+    ("pass", "far", 0, 0), ("finish", 1), ("own", "far", 1, 0), ("own", "mate", 1, 0),
+    ("own", "mate", 1, 1), ("own", "inner", 0, 1), ("own", "near", 1, 1), ("pass", "near", 0, 1),
+    ("pass", "far", 0, 1), ("pass", "far", 1, 0), ("own", "inner", 1, 0), ("pass", "inner", 0, 1),
+    ("own", "far", 1, 1), ("own", "inner", 1, 1), ("pass", "far", 1, 1), ("pass", "near", 1, 0),
+    ("pass", "near", 0, 0), ("pass", "near", 1, 1), ("own", "near", 1, 0), ("beside", 1),
+    ("pass", "inner", 1, 0), ("beside", 0), ("pass", "inner", 1, 1),
+)
+MIDDLE_RELAYS = (True, False)
 F32 = jnp.float32
 BF16 = jnp.bfloat16
 
@@ -79,6 +102,7 @@
     sn,
     rn,
     rm,
+    line,
 ):
     f = lax.axis_index("fs")
     g = lax.axis_index("tp")
@@ -92,7 +116,10 @@
     cols = w.shape[2]
     wide = cols // HEAD * RK
     cut = rz.shape[2]
+    planned = outer == 4 and cut == CUT
     bit = rows // cut
+    fine = r1.shape[2]
+    slip = rows // fine
 
     chunk = max(2 * rows, min(depth, 256))
     chunks = depth // chunk
@@ -126,14 +153,53 @@
     def hello(to):
         pl.semaphore_signal(barrier, inc=1, device_id=to, device_id_type=MESH)
 
+    def at_line(z):
+        return (z * 2 + b, g)
+
     def greet_line(i, c):
-        hello(((a + 1 + i) % outer * 2 + b, g))
+        hello(at_line((a + 1 + i) % outer))
         return c
 
+    chained = outer <= 8
+    below, above = a > 0, a < outer - 1
     hello(mate)
-    lax.fori_loop(0, outer - 1, greet_line, 0)
+    if chained:
+        pl.when(below)(lambda: hello(at_line(a - 1)))
+        pl.when(above)(lambda: hello(at_line(a + 1)))
+        near_by = below.astype(jnp.int32) + above.astype(jnp.int32)
+    else:
+        lax.fori_loop(0, outer - 1, greet_line, 0)
+        near_by = outer - 1
     for i in range(1, t):
         hello((f, (g + i) % t))
+
+    def tell(way, z):
+        pl.semaphore_signal(
+            line.at[way], inc=1, device_id=at_line(z), device_id_type=MESH
+        )
+
+    def tell_neighbours():
+        if chained:
+
+            @pl.when(jnp.logical_and(below, above))
+            def _():
+                tell(0, a - 1)
+                tell(1, a + 1)
+
+    def hear(start, stop):
+        if chained:
+            for way, number, go, to in (
+                (0, outer - 2 - a, below, a - 1),
+                (1, a - 1, above, a + 1),
+            ):
+
+                def pass_along(i, c, way=way, go=go, to=to):
+                    pl.semaphore_wait(line.at[way], 1)
+                    pl.when(go)(lambda: tell(way, to))
+                    return c
+
+                lax.fori_loop(start, jnp.clip(number, start, stop), pass_along, 0)
+
     for x_load in x_loads[1:]:
         x_load.start()
     for i in range(2, 5):
@@ -165,15 +231,21 @@
     def block(z, half):
         return pl.ds(pl.multiple_of((z * 2 + half) * rows, rows), rows)
 
-    def first_copy(k, i, p):
+    def first_copy(k, i, p, h):
         z = flip(at, order[k]) * pairs + i
+        there = pl.ds(h * slip, slip)
         return remote(
-            part.at[p, block(z, 1 - b)],
-            arrived1.at[p, z],
+            part.at[p, pl.ds(pl.multiple_of((z * 2 + 1 - b) * rows + h * slip, slip), slip)],
+            arrived1.at[p, z, there],
             s1.at[p],
-            r1.at[k * pairs + i, p],
+            r1.at[k * pairs + i, p, h],
             mate,
         )
+
+    def first_starts(k, p):
+        for i in range(pairs):
+            for h in range(fine):
+                first_copy(k, i, p, h).start()
 
     def multiply(here):
         sums = lax.dot_general(
@@ -183,35 +255,46 @@
             part[p, here] = sums[:, p * wide : (p + 1) * wide]
 
     apart = rows % 128 == 0
+    order_of = (list(range(chunks)), list(range(chunks)))
+    if VSWAP and chunks == 4:
+        order_of = (order_of[0], [2, 0, 1, 3])
     for k in range(chunks):
         x_loads[k].wait()
         multiply(block(flip(at, order[k]), 1 - b) if apart else chunk_at(k))
         if k == 0:
-            pl.semaphore_wait(barrier, outer + t - 1)
-        for i in range(pairs):
-            first_copy(k, i, 0).start()
-    for k in range(chunks):
-        for i in range(pairs):
-            first_copy(k, i, 1).start()
+            pl.semaphore_wait(barrier, near_by + t)
+        first_starts(k, 0)
+        if k == 0:
+            tell_neighbours()
+    for k in order_of[1]:
+        first_starts(k, 1)
+    hear(0, 1)
     if apart:
         for k in range(chunks):
             multiply(block(flip(at, order[k]), b))
 
     def onward(k, p):
         for i in range(pairs):
-            first_copy(k, i, p).wait_recv()
-            if k < chunks - 1 or pairs > 1:
-                z = flip(at, order[k]) * pairs + i
-                send = remote(
-                    summed.at[p, z], arrived2.at[p, a], s2.at[p], r2.at[p], (z * 2 + b, g)
-                )
-                summed[p, z] = (
-                    part[p, block(z, b)].astype(F32) + arrived1[p, z].astype(F32)
-                ).astype(BF16)
-                if k < chunks - 1:
-                    send.start()
-                else:
-                    pl.when(z != a)(send.start)
+            z = flip(at, order[k]) * pairs + i
+            for h in range(fine):
+                first_copy(k, i, p, h).wait_recv()
+                if k < chunks - 1 or pairs > 1:
+                    there = pl.ds(h * slip, slip)
+                    send = remote(
+                        summed.at[p, z, there],
+                        arrived2.at[p, a, there],
+                        s2.at[p],
+                        r2.at[p],
+                        (z * 2 + b, g),
+                    )
+                    mine = pl.ds(pl.multiple_of((z * 2 + b) * rows + h * slip, slip), slip)
+                    summed[p, z, there] = (
+                        part[p, mine].astype(F32) + arrived1[p, z, there].astype(F32)
+                    ).astype(BF16)
+                    if k < chunks - 1:
+                        send.start()
+                    else:
+                        pl.when(z != a)(send.start)
 
     def others(ref, p):
         return ref.at[p, pl.ds(0, outer - 1)]
@@ -293,19 +376,27 @@
         for i, d in enumerate((2, -2, 1, -1)):
             yield i, d, a + d <= outer - 1 if d > 0 else a + d >= 0
 
-    def finish(p):
+    def scaled(p):
         all_totals(p).wait_recv()
         mean = jnp.sum(jnp.sum(tot_all[p], axis=0), axis=1, keepdims=True) / entries
         scale = 1.0 / jnp.sqrt(mean + 0.25)
         move = scale * raw[p]
         fresh = w[p] - 0.1 * move
         copy[p, block(a, b)] = fresh.astype(BF16)
+
+        def keep():
+            step[p] = move
+            new[p] = fresh
+
+        return keep
+
+    def finish(p):
+        keep = scaled(p)
         for h in range(cut):
             for i, d, ok in own_ways():
                 pl.when(ok)(line_copy(a, p, h, so.at[i, p], a + d).start)
             (own_across(b, h) if p else across(a, b, p, h)).start()
-        step[p] = move
-        new[p] = fresh
+        keep()
 
     def whole(z, p, sem):
         ref = copy.at[p, block(z, b)]
@@ -332,7 +423,7 @@
             pl.when(z >= 0 if far > 0 else z <= outer - 1)(handle)
 
     def sent(p):
-        remote(arrived1.at[p], arrived1.at[p], s1.at[p], r1.at[0, p], mate).wait_send()
+        remote(arrived1.at[p], arrived1.at[p], s1.at[p], rn.at[0], mate).wait_send()
         remote(others(summed, p), others(arrived2, p), s2.at[p], r2.at[p], mate).wait_send()
         all_totals(p).wait_send()
 
@@ -347,36 +438,87 @@
                 pl.when(jnp.logical_and(ok, there))(whole(z, p, sem.at[p]).wait_send)
         crossed(p, outer - p).wait_send()
 
-    for k in range(chunks):
+    onward(0, 0)
+    hear(1, outer)
+    for k in range(1, chunks):
         onward(k, 0)
-    onward(0, 1)
+    onward(order_of[1][0], 1)
     gather(0)
-    for k in range(1, chunks):
+    for k in order_of[1][1:]:
         onward(k, 1)
-    gather(1)
-    finish(0)
-
-    def due(d, p, h):
-        return 4.7 * p + (4.5 + 1.4 * h if d == 1 else 5.2 + 4 * (d - 2) + 3.8 * h)
-
-    def pass_on(h):
-        own_across(1 - b, h).wait_recv()
-        beside(a, h).start()
-
-    todo = [(4.6, lambda: finish(1)), (9, lambda: sent(0)), (9, lambda: sent(1))]
-    for h in range(cut):
-        for d in range(1, outer):
-            for p in range(2):
-                todo.append((due(d, p, h), functools.partial(forward, d, p, h)))
-        todo.append((due(2, 1, h) + 0.1, functools.partial(pass_on, h)))
-    todo.append((due(outer - 1, 1, cut - 1) - 0.1, lambda: sent_copies(0)))
-    for _, act in sorted(todo, key=lambda item: item[0]):
-        act()
-
-    crossed(0, outer).wait_recv()
-    if outer > 2:
+    def play(plan, inward, at_end):
+        later = []
+        away = {"near": 1, "mid": 2, "end": 3} if at_end else {"near": -1, "inner": 1, "far": 2}
+        reach = dict(away, far=2)
+        for i, (kind, *rest) in enumerate(plan):
+            if kind in ("pass", "beside") or i == len(plan) - 1:
+                while later:
+                    later.pop()()
+            if i == len(plan) - 3:
+                sent(0)
+                sent(1)
+            if kind == "gather":
+                gather(1)
+            elif kind == "finish":
+                later.append(scaled(rest[0]))
+            elif kind == "beside":
+                own_across(1 - b, rest[0]).wait_recv()
+                beside(a, rest[0]).start()
+            elif rest[0] == "mate":
+                _, p, h = rest
+                (own_across(b, h) if p else across(a, b, p, h)).start()
+            elif kind == "own":
+                way, p, h = rest
+                line_copy(a, p, h, so.at[0, p], a + inward * reach[way]).start()
+            else:
+                way, p, h = rest
+                z = a + inward * away[way]
+                line_copy(z, p, h, sn.at[0], a).wait_recv()
+                if not at_end and (way == "far" or way == "inner" and MIDDLE_RELAYS[p]):
+                    line_copy(z, p, h, so.at[0, p], a - inward).start()
+                if p == 0 or way != "near":
+                    across(z, b, p, h).start()
+
+    def z_sent(p):
+        for blocks, here in ((2, at_end), (4, jnp.logical_not(at_end))):
+            ref = copy.at[p, pl.ds(0, blocks * rows)]
+            pl.when(here)(remote(ref, ref, so.at[0, p], rn.at[0], mate).wait_send)
+
+    if planned:
+        inward = jnp.where(a < outer // 2, 1, -1)
+        at_end = jnp.logical_or(a == 0, a == outer - 1)
+        pl.when(at_end)(lambda: play(END_PLAN, inward, True))
+        pl.when(jnp.logical_not(at_end))(lambda: play(MIDDLE_PLAN, inward, False))
+        z_sent(0)
+        crossed(0, outer).wait_send()
+        crossed(0, outer).wait_recv()
         crossed(1, outer - 2).wait_recv()
-    sent_copies(1)
+        z_sent(1)
+        crossed(1, outer - 1).wait_send()
+    else:
+        gather(1)
+        finish(0)
+
+        def due(d, p, h):
+            return 4.7 * p + (4.5 + 1.4 * h if d == 1 else 5.2 + 4 * (d - 2) + 3.8 * h)
+
+        def pass_on(h):
+            own_across(1 - b, h).wait_recv()
+            beside(a, h).start()
+
+        todo = [(4.6, lambda: finish(1)), (9, lambda: sent(0)), (9, lambda: sent(1))]
+        for h in range(cut):
+            for d in range(1, outer):
+                for p in range(2):
+                    todo.append((due(d, p, h), functools.partial(forward, d, p, h)))
+            todo.append((due(2, 1, h) + 0.1, functools.partial(pass_on, h)))
+        todo.append((due(outer - 1, 1, cut - 1) - 0.1, lambda: sent_copies(0)))
+        for _, act in sorted(todo, key=lambda item: item[0]):
+            act()
+        crossed(0, outer).wait_recv()
+        if outer > 2:
+            crossed(1, outer - 2).wait_recv()
+        sent_copies(1)
     whole_beside().wait_recv()
     whole_beside().wait_send()
 
@@ -399,6 +541,8 @@
     outer = n // 2
     chunks = depth // max(2 * rows, min(depth, 256))
     cut = CUT if rows % (16 * CUT) == 0 else 1
+    planned = outer == 4 and cut == CUT
+    fine = FINE if rows % (16 * FINE) == 0 else 1
     hbm = pl.BlockSpec(memory_space=pltpu.HBM)
     vmem = pl.BlockSpec(memory_space=pltpu.VMEM)
     shape = jax.ShapeDtypeStruct
@@ -433,19 +577,20 @@
             dma((5,)),
             dma((chunks,)),
             dma((2,)),
-            dma((outer, 2)),
+            dma((outer, 2, fine)),
             dma((2,)),
             dma((2,)),
             dma((2,)),
             dma((2,)),
-            dma((4, 2)),
-            dma((2, max(outer - 3, 1), 2)),
+            dma((1 if planned else 4, 2)),
+            dma((1, 1, 1) if planned else (2, max(outer - 3, 1), 2)),
             dma((outer, 2, cut)),
             dma((2,)),
             dma((2,)),
             dma((1,)),
             dma((1,)),
             dma((cut,)),
+            pltpu.SemaphoreType.REGULAR((2,)),
         ],
         compiler_params=pltpu.CompilerParams(
             collective_id=0, has_side_effects=True, vmem_limit_bytes=62 * 10**6

time: 51 us -> 47 us (0.922)
  Pallas kernels: 50.1 us -> 46.2 us
    pallas_call x1, Pallas kernels: 48.2 us -> 44.2 us  [per_device(): pl.pallas_call(functools.partial(body, n, t), out_shape=kept, in_specs=[h...]
where the time goes in v2:
time: 47 us; the launch traced here: 46.8 us
  Pallas kernels  46.2 us (98%)
  between operations  0.65 us (1%)
    pallas_call x1, Pallas kernels, per_device(): pl.pallas_call(functools.partial(body, n, t), out_shape=kept, in_specs=[h...  44.2 us
    pallas_call x1, Pallas kernels, per_device(): pl.pallas_call(store, out_shape=(full,) * 4 + (whole,) * 2 + (half,) * 4,...  1.91 us

profile of v2, /device:TPU:0, one launch (start us, length us, event | category | flops | bytes accessed | tf_op | source)
XLA Modules:
  0.0 46.8 jit_solution(8240946645619333636)
XLA Ops:
  0.6 44.2 %update.1 = (f32[2,256,256]{2,1,0:T(8,128)S(1)}, f32[2,256,256]{2,1,0:T(8,128)S(1)}, bf16[2,2048,256]{2,1,0:T(8,128)(2,1)S(1)}, f32[2,256,128]{2,1,0:T(8,128)S(1)}, f32[2,256,128]{2,1,0:T(8,128)S(1)}) custom-call(bf16[576,2048]{1,0:T(8,128)(2,1)} %x_hbm.1, bf16[576,256]{1,0:T(8,128)(2,1)} %cq_hbm.1, bf16[576,256]{1,0:T(8,128)(2,1)} %cv_hbm.1, ...), custom_call_target="tpu_custom_call" | custom-call | tf_op jit(solution)/shard_map/update/pallas_call | solution.py:557
  44.9 1.9 %store.1 = (f32[256,256]{1,0:T(8,128)}, f32[256,256]{1,0:T(8,128)}, f32[256,256]{1,0:T(8,128)}, f32[256,256]{1,0:T(8,128)}, bf16[2048,256]{1,0:T(8,128)(2,1)}, /...) custom-call(f32[2,256,256]{2,1,0:T(8,128)S(1)} %get-tuple-element.25, ...), custom_call_target="tpu_custom_call" | custom-call | tf_op jit(solution)/shard_map/store/pallas_call | solution.py:602

commit v3 on v2

--- a/solution.py
+++ b/solution.py
@@ -10,28 +10,26 @@
 HEAD = 64
 RK = 32
 CUT = 2
-FINE = 2
-VSWAP = False
 MESH = pl.DeviceIdType.MESH
 END_PLAN = (
-    ("finish", 0), ("own", "mate", 0, 1), ("own", "mate", 0, 0), ("gather", 1),
-    ("own", "near", 0, 1), ("own", "far", 0, 0), ("pass", "near", 0, 1), ("own", "far", 0, 1),
-    ("pass", "near", 0, 0), ("finish", 1), ("own", "mate", 1, 1), ("own", "mate", 1, 0),
-    ("own", "far", 1, 0), ("own", "near", 0, 0), ("pass", "mid", 0, 0), ("own", "far", 1, 1),
-    ("own", "near", 1, 1), ("pass", "end", 0, 0), ("own", "near", 1, 0), ("pass", "mid", 1, 0),
-    ("pass", "near", 1, 1), ("beside", 0), ("pass", "end", 0, 1), ("pass", "end", 1, 0),
-    ("beside", 1), ("pass", "mid", 0, 1), ("pass", "mid", 1, 1), ("pass", "end", 1, 1),
-    ("pass", "near", 1, 0),
+    ("finish", 0), ("own", "near", 0, 0), ("own", "mate", 0, 1), ("own", "mate", 0, 0),
+    ("gather", 1), ("own", "near", 0, 1), ("pass", "near", 0, 1), ("own", "far", 0, 1),
+    ("pass", "near", 0, 0), ("own", "far", 0, 0), ("pass", "mid", 0, 0), ("finish", 1),
+    ("own", "mate", 1, 0), ("own", "mate", 1, 1), ("own", "far", 1, 1), ("own", "far", 1, 0),
+    ("pass", "mid", 0, 1), ("own", "near", 1, 1), ("pass", "end", 0, 1), ("pass", "mid", 1, 1),
+    ("pass", "mid", 1, 0), ("own", "near", 1, 0), ("pass", "near", 1, 0), ("pass", "end", 1, 1),
+    ("beside", 1), ("pass", "end", 0, 0), ("beside", 0), ("pass", "end", 1, 0),
+    ("pass", "near", 1, 1),
 )
 MIDDLE_PLAN = (
-    ("finish", 0), ("own", "mate", 0, 0), ("own", "mate", 0, 1), ("gather", 1),
-    ("own", "near", 0, 1), ("own", "inner", 0, 0), ("own", "near", 0, 0), ("pass", "inner", 0, 0),
-    ("pass", "far", 0, 0), ("finish", 1), ("own", "far", 1, 0), ("own", "mate", 1, 0),
-    ("own", "mate", 1, 1), ("own", "inner", 0, 1), ("own", "near", 1, 1), ("pass", "near", 0, 1),
-    ("pass", "far", 0, 1), ("pass", "far", 1, 0), ("own", "inner", 1, 0), ("pass", "inner", 0, 1),
-    ("own", "far", 1, 1), ("own", "inner", 1, 1), ("pass", "far", 1, 1), ("pass", "near", 1, 0),
-    ("pass", "near", 0, 0), ("pass", "near", 1, 1), ("own", "near", 1, 0), ("beside", 1),
-    ("pass", "inner", 1, 0), ("beside", 0), ("pass", "inner", 1, 1),
+    ("finish", 0), ("own", "inner", 0, 0), ("own", "near", 0, 1), ("own", "mate", 0, 1),
+    ("own", "inner", 0, 1), ("own", "mate", 0, 0), ("own", "near", 0, 0), ("gather", 1),
+    ("pass", "inner", 0, 0), ("pass", "inner", 0, 1), ("pass", "near", 0, 1),
+    ("pass", "near", 0, 0), ("finish", 1), ("own", "far", 1, 1), ("pass", "far", 0, 1),
+    ("own", "near", 1, 0), ("own", "mate", 1, 0), ("own", "far", 1, 0), ("pass", "far", 0, 0),
+    ("own", "mate", 1, 1), ("pass", "far", 1, 1), ("pass", "far", 1, 0), ("own", "inner", 1, 0),
+    ("pass", "near", 1, 1), ("own", "inner", 1, 1), ("own", "near", 1, 1), ("beside", 0),
+    ("pass", "inner", 1, 0), ("pass", "inner", 1, 1), ("beside", 1), ("pass", "near", 1, 0),
 )
 MIDDLE_RELAYS = (True, False)
 F32 = jnp.float32
@@ -96,7 +94,6 @@
     rt,
     so,
     sr,
-    rz,
     sy,
     ry,
     sn,
@@ -115,7 +112,8 @@
     rows = depth // n
     cols = w.shape[2]
     wide = cols // HEAD * RK
-    cut = rz.shape[2]
+    cut = r1.shape[2]
+    rz = r1
     planned = outer == 4 and cut == CUT
     bit = rows // cut
     fine = r1.shape[2]
@@ -256,8 +254,8 @@
 
     apart = rows % 128 == 0
     order_of = (list(range(chunks)), list(range(chunks)))
-    if VSWAP and chunks == 4:
-        order_of = (order_of[0], [2, 0, 1, 3])
+    if chunks == 4:
+        order_of = (order_of[0], [0, 2, 1, 3])
     for k in range(chunks):
         x_loads[k].wait()
         multiply(block(flip(at, order[k]), 1 - b) if apart else chunk_at(k))
@@ -442,9 +440,8 @@
     hear(1, outer)
     for k in range(1, chunks):
         onward(k, 0)
-    onward(order_of[1][0], 1)
     gather(0)
-    for k in order_of[1][1:]:
+    for k in order_of[1]:
         onward(k, 1)
     def play(plan, inward, at_end):
         later = []
@@ -542,7 +539,7 @@
     chunks = depth // max(2 * rows, min(depth, 256))
     cut = CUT if rows % (16 * CUT) == 0 else 1
     planned = outer == 4 and cut == CUT
-    fine = FINE if rows % (16 * FINE) == 0 else 1
+    fine = cut
     hbm = pl.BlockSpec(memory_space=pltpu.HBM)
     vmem = pl.BlockSpec(memory_space=pltpu.VMEM)
     shape = jax.ShapeDtypeStruct
@@ -584,7 +581,6 @@
             dma((2,)),
             dma((1 if planned else 4, 2)),
             dma((1, 1, 1) if planned else (2, max(outer - 3, 1), 2)),
-            dma((outer, 2, cut)),
             dma((2,)),
             dma((2,)),
             dma((1,)),

time: 47 us -> 46.3 us (0.985)
  Pallas kernels: 46.2 us -> 45.4 us
    pallas_call x1, Pallas kernels: 44.2 us -> 43.5 us  [per_device(): pl.pallas_call(functools.partial(body, n, t), out_shape=kept, in_specs=[h...]
where the time goes in v3:
time: 46.3 us; the launch traced here: 46 us
  Pallas kernels  45.4 us (98%)
  between operations  0.65 us (1%)
    pallas_call x1, Pallas kernels, per_device(): pl.pallas_call(functools.partial(body, n, t), out_shape=kept, in_specs=[h...  43.5 us
    pallas_call x1, Pallas kernels, per_device(): pl.pallas_call(store, out_shape=(full,) * 4 + (whole,) * 2 + (half,) * 4,...  1.91 us

profile of v3, /device:TPU:0, one launch (start us, length us, event | category | flops | bytes accessed | tf_op | source)
XLA Modules:
  0.0 46.0 jit_solution(13653724322161663532)
XLA Ops:
  0.6 43.5 %update.1 = (f32[2,256,256]{2,1,0:T(8,128)S(1)}, f32[2,256,256]{2,1,0:T(8,128)S(1)}, bf16[2,2048,256]{2,1,0:T(8,128)(2,1)S(1)}, f32[2,256,128]{2,1,0:T(8,128)S(1)}, f32[2,256,128]{2,1,0:T(8,128)S(1)}) custom-call(bf16[576,2048]{1,0:T(8,128)(2,1)} %x_hbm.1, bf16[576,256]{1,0:T(8,128)(2,1)} %cq_hbm.1, bf16[576,256]{1,0:T(8,128)(2,1)} %cv_hbm.1, ...), custom_call_target="tpu_custom_call" | custom-call | tf_op jit(solution)/shard_map/update/pallas_call | solution.py:554
  44.1 1.9 %store.1 = (f32[256,256]{1,0:T(8,128)}, f32[256,256]{1,0:T(8,128)}, f32[256,256]{1,0:T(8,128)}, f32[256,256]{1,0:T(8,128)}, bf16[2048,256]{1,0:T(8,128)(2,1)}, /...) custom-call(f32[2,256,256]{2,1,0:T(8,128)S(1)} %get-tuple-element.25, ...), custom_call_target="tpu_custom_call" | custom-call | tf_op jit(solution)/shard_map/store/pallas_call | solution.py:598

commit v4 on v3

--- a/solution.py
+++ b/solution.py
@@ -12,13 +12,13 @@
 CUT = 2
 MESH = pl.DeviceIdType.MESH
 END_PLAN = (
-    ("finish", 0), ("own", "near", 0, 0), ("own", "mate", 0, 1), ("own", "mate", 0, 0),
-    ("gather", 1), ("own", "near", 0, 1), ("pass", "near", 0, 1), ("own", "far", 0, 1),
+    ("finish", 0), ("own", "near", 0, 0), ("own", "mate", 0, 1), ("gather", 1),
+    ("own", "mate", 0, 0), ("own", "near", 0, 1), ("pass", "near", 0, 1), ("own", "far", 0, 1),
     ("pass", "near", 0, 0), ("own", "far", 0, 0), ("pass", "mid", 0, 0), ("finish", 1),
     ("own", "mate", 1, 0), ("own", "mate", 1, 1), ("own", "far", 1, 1), ("own", "far", 1, 0),
     ("pass", "mid", 0, 1), ("own", "near", 1, 1), ("pass", "end", 0, 1), ("pass", "mid", 1, 1),
-    ("pass", "mid", 1, 0), ("own", "near", 1, 0), ("pass", "near", 1, 0), ("pass", "end", 1, 1),
-    ("beside", 1), ("pass", "end", 0, 0), ("beside", 0), ("pass", "end", 1, 0),
+    ("pass", "end", 0, 0), ("pass", "mid", 1, 0), ("own", "near", 1, 0), ("pass", "near", 1, 0),
+    ("pass", "end", 1, 1), ("beside", 1), ("beside", 0), ("pass", "end", 1, 0),
     ("pass", "near", 1, 1),
 )
 MIDDLE_PLAN = (
@@ -26,8 +26,8 @@
     ("own", "inner", 0, 1), ("own", "mate", 0, 0), ("own", "near", 0, 0), ("gather", 1),
     ("pass", "inner", 0, 0), ("pass", "inner", 0, 1), ("pass", "near", 0, 1),
     ("pass", "near", 0, 0), ("finish", 1), ("own", "far", 1, 1), ("pass", "far", 0, 1),
-    ("own", "near", 1, 0), ("own", "mate", 1, 0), ("own", "far", 1, 0), ("pass", "far", 0, 0),
-    ("own", "mate", 1, 1), ("pass", "far", 1, 1), ("pass", "far", 1, 0), ("own", "inner", 1, 0),
+    ("pass", "far", 0, 0), ("own", "near", 1, 0), ("own", "mate", 1, 0), ("pass", "far", 1, 1),
+    ("own", "far", 1, 0), ("own", "mate", 1, 1), ("pass", "far", 1, 0), ("own", "inner", 1, 0),
     ("pass", "near", 1, 1), ("own", "inner", 1, 1), ("own", "near", 1, 1), ("beside", 0),
     ("pass", "inner", 1, 0), ("pass", "inner", 1, 1), ("beside", 1), ("pass", "near", 1, 0),
 )

time: 46.3 us -> 46 us (level)
  no operation moved by 1% of the time
where the time goes in v4:
time: 46 us; the launch traced here: 45.8 us
  Pallas kernels  45.1 us (98%)
  between operations  0.65 us (1%)
    pallas_call x1, Pallas kernels, per_device(): pl.pallas_call(functools.partial(body, n, t), out_shape=kept, in_specs=[h...  43.2 us
    pallas_call x1, Pallas kernels, per_device(): pl.pallas_call(store, out_shape=(full,) * 4 + (whole,) * 2 + (half,) * 4,...  1.91 us

profile of v4, /device:TPU:0, one launch (start us, length us, event | category | flops | bytes accessed | tf_op | source)
XLA Modules:
  0.0 45.8 jit_solution(933979235313519852)
XLA Ops:
  0.6 43.2 %update.1 = (f32[2,256,256]{2,1,0:T(8,128)S(1)}, f32[2,256,256]{2,1,0:T(8,128)S(1)}, bf16[2,2048,256]{2,1,0:T(8,128)(2,1)S(1)}, f32[2,256,128]{2,1,0:T(8,128)S(1)}, f32[2,256,128]{2,1,0:T(8,128)S(1)}) custom-call(bf16[576,2048]{1,0:T(8,128)(2,1)} %x_hbm.1, bf16[576,256]{1,0:T(8,128)(2,1)} %cq_hbm.1, bf16[576,256]{1,0:T(8,128)(2,1)} %cv_hbm.1, ...), custom_call_target="tpu_custom_call" | custom-call | tf_op jit(solution)/shard_map/update/pallas_call | solution.py:554
  43.9 1.9 %store.1 = (f32[256,256]{1,0:T(8,128)}, f32[256,256]{1,0:T(8,128)}, f32[256,256]{1,0:T(8,128)}, f32[256,256]{1,0:T(8,128)}, bf16[2048,256]{1,0:T(8,128)(2,1)}, /...) custom-call(f32[2,256,256]{2,1,0:T(8,128)S(1)} %get-tuple-element.25, ...), custom_call_target="tpu_custom_call" | custom-call | tf_op jit(solution)/shard_map/store/pallas_call | solution.py:598
